TPU v7x, 128 devices: a whole 4x4x4 slice. The times are simulated.
128 devices in a mesh: ra: 16 (over z, x), cb: 8 (over y, core).
Axes of the slice: x: 4, y: 4, z: 4, core: 2. Of those that a mesh axis runs over, the one named last changes fastest.
Arguments:
- inputs: bfloat16 [1536, 4096], P(None, 'ra'), may hold values from -12 to 12
- gate_weight: bfloat16 [2, 4096, 11264], P(None, 'ra', 'cb'), may hold values from -0.09375 to 0.09375
- up_weight: bfloat16 [2, 4096, 11264], P(None, 'ra', 'cb'), may hold values from -0.09375 to 0.09375
- down_weight: bfloat16 [2, 11264, 4096], P(None, 'cb', 'ra'), may hold values from -0.0546875 to 0.0546875
- norm_gain: float32 [2, 4096], P(None, 'ra'), may hold values from 0.05 to 8
- norm_shift: float32 [2, 4096], P(None, 'ra'), may hold values from -1.5 to 1.5
Outputs:
- outputs: bfloat16 [1536, 4096], P(None, 'ra')
All inputs are finite; a program needn't handle non-finite values.
Results may differ from a plain program's by a relative error of at most 0.04.
Values may be sent and summed in bfloat16 or wider, within the bound.
No kernel may reach another device: no remote copies, remote signals or barrier semaphores. Data moves between devices by JAX's collectives and lax.ppermute only.
A program may use at most 64 MiB of HBM per device.

v0:
```python
import functools

import jax
import jax.numpy as jnp
from jax import lax
from jax.sharding import Mesh
from jax.sharding import PartitionSpec as P

LAYERS = 2
RA = ("ra_0", "ra_1")


RESIDUAL = 0.5
EPSILON = 1e-05


def in_blocks(shard, dim, peers):
    lengths = shard.shape
    parts = shard.reshape(*lengths[:dim], peers, lengths[dim] // peers, *lengths[dim + 1 :])
    return jnp.moveaxis(parts, dim, 0)


def sum_at_owner(shard, axis, dim):
    parts = in_blocks(shard, dim, lax.axis_size(axis))
    arrived = lax.all_to_all(parts, axis, split_axis=0, concat_axis=0, tiled=True)
    return arrived.astype(jnp.float32).sum(axis=0)


def over_axes(shard, axes):
    return functools.reduce(lax.psum, axes, shard)


def from_everyone(shard, axis):
    peers = lax.axis_size(axis)
    return lax.all_to_all(
        jnp.broadcast_to(shard[None], (peers, *shard.shape)), axis, 0, 0, tiled=True
    )


def in_order(parts, dim):
    parts = jnp.moveaxis(parts, 0, dim)
    lengths = parts.shape
    return parts.reshape(*lengths[:dim], lengths[dim] * lengths[dim + 1], *lengths[dim + 2 :])


def collect(shard, axis, dim):
    parts = from_everyone(shard, axis)
    return in_order(parts, dim)


def scale_rows(mixed_rows, row_sum, row_squares, gain_row, shift_row, full_width):
    mean_rows = row_sum / full_width
    var_rows = row_squares / full_width - mean_rows * mean_rows
    normed = (mixed_rows - mean_rows[:, None]) * lax.rsqrt(var_rows + EPSILON)[:, None]
    return (normed * gain_row + shift_row).astype(jnp.bfloat16)


def sublayer(stream, w_gate, w_up, w_down, gain_row, shift_row):
    columns = w_gate.shape[1]
    paired = jnp.concatenate((w_gate, w_up), axis=1)
    full_width = stream.shape[1] * lax.axis_size(RA)
    summed = lax.psum_scatter(
        jnp.dot(stream, paired, preferred_element_type=jnp.float32).astype(jnp.bfloat16),
        RA,
        scatter_dimension=0,
        tiled=True,
    ).astype(jnp.float32)
    hidden = (jax.nn.silu(summed[:, :columns]) * summed[:, columns:]).astype(jnp.bfloat16)
    partial_value = jnp.dot(
        lax.all_gather(hidden, RA, axis=0, tiled=True), w_down, preferred_element_type=jnp.float32
    )
    branch = sum_at_owner(partial_value.astype(jnp.bfloat16), "cb", 0)
    row_count = branch.shape[0]
    own_rows = lax.dynamic_slice_in_dim(stream, lax.axis_index("cb") * row_count, row_count, 0)
    mixed_rows = RESIDUAL * own_rows.astype(jnp.float32) + branch
    row_sum, row_squares = (
        over_axes(jnp.sum(mixed_rows, axis=1), RA),
        over_axes(jnp.sum(mixed_rows * mixed_rows, axis=1), RA),
    )
    normed = scale_rows(mixed_rows, row_sum, row_squares, gain_row, shift_row, full_width)
    return collect(normed, "cb", 0)


def per_device(inputs, gate_weight, up_weight, down_weight, norm_gain, norm_shift):
    stream = inputs
    for layer_index in range(LAYERS):
        stream = sublayer(
            stream,
            gate_weight[layer_index],
            up_weight[layer_index],
            down_weight[layer_index],
            norm_gain[layer_index],
            norm_shift[layer_index],
        )
    return stream


def solution(mesh):
    finer = Mesh(mesh.devices.reshape(4, 4, mesh.shape["cb"]), ("ra_0", "ra_1", "cb"))
    in_specs = (
        P(None, RA),
        P(None, RA, "cb"),
        P(None, RA, "cb"),
        P(None, "cb", RA),
        P(None, RA),
        P(None, RA),
    )
    out_specs = P(None, RA)
    return jax.shard_map(
        per_device, mesh=finer, in_specs=in_specs, out_specs=out_specs, check_vma=False
    )
```

profile of v0, /device:TPU:1, one launch (start us, length us, event | category | flops | bytes accessed | tf_op | source)
XLA Modules:
  0.0 432.4 jit_solution(12249550608006333865)
XLA Ops:
  6.5 2.0 slice_bitcast_fusion
  8.6 5.8 %fusion = bf16[1536,2816]{0,1:T(8,128)(2,1)} fusion(bf16[1536,256]{1,0:T(8,128)(2,1)S(1)} %copy-done, bf16[256,1408]{1,0:T(8,128)(2,1)S(1)} %get-tuple-element.20, bf16[256,1408]{1,0:T(8,128)(2,1)S(1)} %get-tuple-element.29), kind=kOutput, calls=%fused_computation.2 | convolution fusion | flops 2221801472 | bytes 10878976 | tf_op jit(solution)/shard_map/dot_general | solution.py:63
  14.4 11.5 %copy.11 = bf16[1536,2816]{1,0:T(8,128)(2,1)} copy(bf16[1536,2816]{0,1:T(8,128)(2,1)} %fusion) | data formatting | bytes 17301504
  26.0 88.4 %reduce-scatter.7.cloned.1.call-done = bf16[96,2816]{1,0:T(8,128)(2,1)} async-done(((bf16[1536,2816]{1,0:T(8,128)(2,1)}), bf16[96,2816]{1,0:T(8,128)(2,1)}) %reduce-scatter.7.cloned.1.call-update) | async-done | bytes 540688
  114.4 1.4 copy.12
  115.9 0.2 fusion.8
  116.1 0.9 copy.8
  117.0 52.8 %all-gather.3.cloned.1.call-done = bf16[1536,1408]{1,0:T(8,128)(2,1)} async-done(((bf16[96,1408]{1,0:T(8,128)(2,1)}), bf16[1536,1408]{1,0:T(8,128)(2,1)}) %all-gather.3.cloned.1.call-update) | async-done | bytes 4325392 | tf_op jit(solution)/shard_map/all_gather | solution.py:70
  169.8 4.7 %convolution_convert_fusion.3 = bf16[1536,256]{1,0:T(8,128)(2,1)} fusion(bf16[1536,1408]{1,0:T(8,128)(2,1)} %all-gather.3.cloned.1.call-done, bf16[2,1408,256]{2,1,0:T(8,128)(2,1)} %param.9), kind=kOutput, calls=%fused_computation.4 | convolution fusion | flops 1107689472 | bytes 5832704 | tf_op jit(solution)/shard_map/dot_general | solution.py:69
  174.5 5.3 %all-to-all-start = ((bf16[8,192,256]{2,1,0:T(8,128)(2,1)}), bf16[8,192,256]{2,1,0:T(8,128)(2,1)S(1)}, u32[]{:S(2)}, u32[]{:S(2)}) async-start(bf16[8,192,256]{2,1,0:T(8,128)(2,1)} %bitcast.34), calls=%async_computation | async-start | bytes 1572864 | tf_op jit(solution)/shard_map/all_to_all | solution.py:25
  179.8 12.1 %all-to-all-done = bf16[8,192,256]{2,1,0:T(8,128)(2,1)S(1)} async-done(((bf16[8,192,256]{2,1,0:T(8,128)(2,1)}), bf16[8,192,256]{2,1,0:T(8,128)(2,1)S(1)}, u32[]{:S(2)}, u32[]{:S(2)}) %all-to-all-start) | async-done | bytes 786464 | tf_op jit(solution)/shard_map/all_to_all | solution.py:25
  191.9 0.1 convert_reduce_fusion.1
  192.0 0.2 fusion.13
  192.2 8.4 %all-reduce.3 = (f32[192]{0:T(256)S(1)}, f32[192]{0:T(256)S(1)}) all-reduce(f32[192]{0:T(256)S(1)} %get-tuple-element.8, f32[192]{0:T(256)S(1)} %get-tuple-element.7), channel_id=1, replica_groups=mesh['ra_0'=4,'ra_1'=4,'cb'=8] {'ra_0'}, use_global_device_ids=true, to_apply=%region_6.7 | all-reduce | flops 384 | bytes 3072 | tf_op jit(solution)/shard_map/psum | solution.py:30
  200.6 6.7 %all-reduce.1 = (f32[192]{0:T(256)S(1)}, f32[192]{0:T(256)S(1)}) all-reduce(f32[192]{0:T(256)S(1)} %get-tuple-element.15, f32[192]{0:T(256)S(1)} %get-tuple-element.16), channel_id=1, replica_groups=mesh['ra_0'=4,'ra_1'=4,'cb'=8] {'ra_1'}, use_global_device_ids=true, to_apply=%region_7.8 | all-reduce | flops 384 | bytes 3072 | tf_op jit(solution)/shard_map/psum | solution.py:30
  207.3 0.1 add_convert_fusion.1
  207.5 19.4 %all_to_all.20 = bf16[8,192,256]{2,1,0:T(8,128)(2,1)S(1)} all-to-all(bf16[8,192,256]{2,1,0:T(8,128)(2,1)S(1)} %broadcast_in_dim.4), channel_id=1, replica_groups=mesh['ra_0'=4,'ra_1'=4,'cb'=8] {'cb'}, dimensions={0} | all-to-all | bytes 1572864 | tf_op jit(solution)/shard_map/all_to_all | solution.py:35
  226.9 5.7 %convolution_convert_fusion = bf16[1536,2816]{1,0:T(8,128)(2,1)} fusion(bf16[1536,256]{1,0:T(8,128)(2,1)S(1)} %bitcast.30, bf16[256,1408]{1,0:T(8,128)(2,1)S(1)} %get-tuple-element.19, bf16[256,1408]{1,0:T(8,128)(2,1)S(1)} %get-tuple-element.30), kind=kOutput, calls=%fused_computation | convolution fusion | flops 2221801472 | bytes 10878976 | tf_op jit(solution)/shard_map/dot_general | solution.py:63
  232.7 81.0 %reduce-scatter.9.cloned.1.call-done = bf16[96,2816]{1,0:T(8,128)(2,1)} async-done(((bf16[1536,2816]{1,0:T(8,128)(2,1)}), bf16[96,2816]{1,0:T(8,128)(2,1)}) %reduce-scatter.9.cloned.1.call-update) | async-done | bytes 540688
  313.7 1.4 copy.14
  315.2 0.2 fusion.7
  315.4 0.9 copy.10
  316.3 52.8 %all-gather.5.cloned.1.call-done = bf16[1536,1408]{1,0:T(8,128)(2,1)} async-done(((bf16[96,1408]{1,0:T(8,128)(2,1)}), bf16[1536,1408]{1,0:T(8,128)(2,1)}) %all-gather.5.cloned.1.call-update) | async-done | bytes 4325392 | tf_op jit(solution)/shard_map/all_gather | solution.py:70
  369.1 3.8 convolution_convert_fusion.2
  372.9 17.1 %all_to_all.21 = bf16[8,192,256]{2,1,0:T(8,128)(2,1)S(1)} all-to-all(bf16[8,192,256]{2,1,0:T(8,128)(2,1)S(1)} %bitcast.35), channel_id=1, replica_groups=mesh['ra_0'=4,'ra_1'=4,'cb'=8] {'cb'}, dimensions={0} | all-to-all | bytes 1572864 | tf_op jit(solution)/shard_map/all_to_all | solution.py:25
  390.0 0.1 convert_reduce_fusion
  390.1 0.2 fusion.14
  390.2 8.4 %all-reduce.2 = (f32[192]{0:T(256)S(1)}, f32[192]{0:T(256)S(1)}) all-reduce(f32[192]{0:T(256)S(1)} %get-tuple-element.6, f32[192]{0:T(256)S(1)} %get-tuple-element.5), channel_id=1, replica_groups=mesh['ra_0'=4,'ra_1'=4,'cb'=8] {'ra_0'}, use_global_device_ids=true, to_apply=%region_14.15 | all-reduce | flops 384 | bytes 3072 | tf_op jit(solution)/shard_map/psum | solution.py:30
  398.6 6.8 %all-reduce = (f32[192]{0:T(256)S(1)}, f32[192]{0:T(256)S(1)}) all-reduce(f32[192]{0:T(256)S(1)} %get-tuple-element.13, f32[192]{0:T(256)S(1)} %get-tuple-element.14), channel_id=1, replica_groups=mesh['ra_0'=4,'ra_1'=4,'cb'=8] {'ra_1'}, use_global_device_ids=true, to_apply=%region_15.16 | all-reduce | flops 384 | bytes 3072 | tf_op jit(solution)/shard_map/psum | solution.py:30
  405.4 0.1 add_convert_fusion
  405.6 19.4 %all_to_all.22 = bf16[8,192,256]{2,1,0:T(8,128)(2,1)S(1)} all-to-all(bf16[8,192,256]{2,1,0:T(8,128)(2,1)S(1)} %broadcast_in_dim.5), channel_id=1, replica_groups=mesh['ra_0'=4,'ra_1'=4,'cb'=8] {'cb'}, dimensions={0} | all-to-all | bytes 1572864 | tf_op jit(solution)/shard_map/all_to_all | solution.py:35
  425.0 0.9 copy.16
  (22 shorter events, 0.5 us)
Async XLA Ops:
  6.5 2.1 copy-start
  6.5 107.8 %reduce-scatter.7.cloned.1.call-start = ((), (), s32[]{:S(2)}) async-start(), calls=%async_computation.8 | async-start | bytes 9191424
  25.9 143.9 %all-gather.3.cloned.1.call-start = ((), (), s32[]{:S(2)}) async-start(), calls=%async_computation.6 | async-start | bytes 4595712 | tf_op jit(solution)/shard_map/all_gather | solution.py:70
  174.5 5.3 %copy-start.1 = (f32[2,256]{1,0:T(2,128)S(1)}, f32[2,256]{1,0:T(2,128)}, u32[]{:S(2)}) copy-start(f32[2,256]{1,0:T(2,128)} %param.10) | copy-start | bytes 6148
  174.5 5.3 %copy-start.2 = (f32[2,256]{1,0:T(2,128)S(1)}, f32[2,256]{1,0:T(2,128)}, u32[]{:S(2)}) copy-start(f32[2,256]{1,0:T(2,128)} %param.11) | copy-start | bytes 6148
  174.5 17.4 %all-to-all-start = ((bf16[8,192,256]{2,1,0:T(8,128)(2,1)}), bf16[8,192,256]{2,1,0:T(8,128)(2,1)S(1)}, u32[]{:S(2)}, u32[]{:S(2)}) async-start(bf16[8,192,256]{2,1,0:T(8,128)(2,1)} %bitcast.34), calls=%async_computation | async-start | bytes 1572864 | tf_op jit(solution)/shard_map/all_to_all | solution.py:25
  179.7 133.9 %reduce-scatter.9.cloned.1.call-start = ((), (), s32[]{:S(2)}) async-start(), calls=%async_computation.9 | async-start | bytes 9191424
  232.6 136.5 %all-gather.5.cloned.1.call-start = ((), (), s32[]{:S(2)}) async-start(), calls=%async_computation.7 | async-start | bytes 4595712 | tf_op jit(solution)/shard_map/all_gather | solution.py:70
Sparse Core Ops, SparseCore 0:
  26.1 88.2 reduce-scatter.6
  117.1 52.6 all-gather.2
  232.7 80.9 reduce-scatter.8
  316.4 52.6 all-gather.4
where the time goes:
time: 433 us; the launch traced here: 432 us
  waiting for transfers between devices  287 us (66%)
  blocking collectives  86.1 us (20%)
  matrix products  20 us (5%)
  local copies, waits for them, and re-layouts  19.1 us (4%)
  between operations  13.3 us (3%)
  starting transfers between devices  5.34 us (1%)
    unnamed x6, waiting for transfers between devices  169 us
    all_gather x2, waiting for transfers between devices, sublayer(): lax.all_gather(hidden, RA, axis=0, tiled=True)  106 us
    all_to_all x2, blocking collectives, from_everyone(): lax.all_to_all(jnp.broadcast_to(shard[None], (peers, *shard.shape)), axis...  38.8 us
    psum x4, blocking collectives, over_axes(): return functools.reduce(lax.psum, axes, shard)  30.3 us
    all_to_all x1, blocking collectives, sum_at_owner(): lax.all_to_all(parts, axis, split_axis=0, concat_axis=0, tiled=True)  17.1 us
    unnamed x10, local copies, waits for them, and re-layouts  15.2 us
    all_to_all x1, waiting for transfers between devices, sum_at_owner(): lax.all_to_all(parts, axis, split_axis=0, concat_axis=0, tiled=True)  12.1 us
    dot_general x2, matrix products, sublayer(): jnp.dot(stream, paired, preferred_element_type=jnp.float32)  11.5 us
  transfers between devices with their start and end apart: 5, of which 5 were waited for; matrix products, arithmetic and copies ran while one was open for 0% of the time, Pallas kernels for 0%

commit v1 on v0

v1 whole, which is shorter than its diff:
```python
import jax
import jax.numpy as jnp
from jax import lax
from jax.sharding import Mesh
from jax.sharding import PartitionSpec as P

RESIDUAL = 0.5
EPSILON = 1e-05
BF16 = jnp.bfloat16
F32 = jnp.float32


def exchange(parts, axes):
    return lax.all_to_all(parts, axes, 0, 0, tiled=True)


def share(block, axes, peers):
    return exchange(jnp.broadcast_to(block[None], (peers, *block.shape)), axes)


def swap_core(block):
    return lax.ppermute(block, "c", [(0, 1), (1, 0)])


def dot_nt(a, b):
    return lax.dot_general(a, b, (((1,), (1,)), ((), ())), preferred_element_type=F32)


def regroup_weights(gate, up, down):
    stacked = jnp.stack((gate.T, up.T, down))
    rows = stacked.shape[1] // 4
    parts = stacked.reshape(3, 4, rows, 256).transpose(1, 0, 2, 3)
    mine = exchange(parts, "x")
    mine = mine.transpose(1, 2, 0, 3).reshape(3, rows, 1024)
    other = swap_core(mine)
    both = jnp.concatenate((mine, other), axis=1)
    return both[:2].reshape(2 * 2 * rows, 1024), both[2]


def normed(mixed, row_sum, row_squares, gain, shift):
    mean = row_sum / 4096.0
    var = row_squares / 4096.0 - mean * mean
    out = (mixed - mean[:, None]) * lax.rsqrt(var + EPSILON)[:, None]
    return (out * gain + shift).astype(BF16)


def hidden_units(stream, w_gu):
    partial = dot_nt(stream, w_gu).astype(BF16)
    cols = partial.shape[1] // 2
    summed = exchange(partial.reshape(4, -1, 2 * cols), "z").astype(F32).sum(axis=0)
    hidden = (jax.nn.silu(summed[:, :cols]) * summed[:, cols:]).astype(BF16)
    return share(hidden, "z", 4).reshape(-1, cols)


def per_device(inputs, gate_weight, up_weight, down_weight, norm_gain, norm_shift):
    c = lax.axis_index("c")
    x = lax.axis_index("x")
    y = lax.axis_index("y")
    half = inputs.shape[0] // 2
    quarter = half // 4
    mine = lax.dynamic_slice_in_dim(inputs, c * half + y * quarter, quarter, 0)
    rows = share(mine, "x", 4).transpose(1, 0, 2).reshape(quarter, 1024)
    stream = share(rows, "y", 4).reshape(half, 1024)
    affine = jnp.stack((norm_gain[0], norm_shift[0]))
    affine = lax.all_gather(affine, "x", axis=1, tiled=True)
    gu0, down0 = regroup_weights(gate_weight[0], up_weight[0], down_weight[0])
    gu1, down1 = regroup_weights(gate_weight[1], up_weight[1], down_weight[1])

    hidden = hidden_units(stream, gu0)
    partial = jnp.dot(hidden, down0, preferred_element_type=F32).astype(BF16)
    block = half // 16
    branch = exchange(partial.reshape(16, block, 1024), ("x", "y")).astype(F32).sum(axis=0)
    own = lax.dynamic_slice_in_dim(stream, (x * 4 + y) * block, block, 0)
    mixed = RESIDUAL * own.astype(F32) + branch
    stats = lax.psum(jnp.stack((mixed.sum(axis=1), (mixed * mixed).sum(axis=1))), "z")
    out = normed(mixed, stats[0], stats[1], affine[0], affine[1])
    stream = share(out, ("x", "y"), 16).reshape(half, 1024)

    hidden = hidden_units(stream, gu1)
    partial = jnp.dot(hidden, down1, preferred_element_type=F32).astype(BF16)
    parts = partial.reshape(4, quarter, 4, 256).transpose(2, 0, 1, 3).reshape(16, quarter, 256)
    branch = exchange(parts, ("x", "y")).astype(F32).sum(axis=0)
    own = lax.dynamic_slice(stream, (y * quarter, x * 256), (quarter, 256))
    mixed = RESIDUAL * own.astype(F32) + branch
    stats = lax.psum(jnp.stack((mixed.sum(axis=1), (mixed * mixed).sum(axis=1))), ("z", "x"))
    out = normed(mixed, stats[0], stats[1], norm_gain[1], norm_shift[1])
    ours = share(out, "y", 4).reshape(half, 256)
    theirs = swap_core(ours)
    result = jnp.concatenate((ours, theirs), axis=0)
    swapped = jnp.concatenate((theirs, ours), axis=0)
    return jnp.where(c == 0, result, swapped)


def solution(mesh):
    finer = Mesh(mesh.devices.reshape(4, 4, 4, 2), ("z", "x", "y", "c"))
    ra, cb = ("z", "x"), ("y", "c")
    in_specs = (
        P(None, ra),
        P(None, ra, cb),
        P(None, ra, cb),
        P(None, cb, ra),
        P(None, ra),
        P(None, ra),
    )
    return jax.shard_map(
        per_device, mesh=finer, in_specs=in_specs, out_specs=P(None, ra), check_vma=False
    )
```

time: 433 us -> 367 us (0.85)
  waiting for transfers between devices: 287 us -> 76.9 us
  blocking collectives: 86.1 us -> 177 us
  starting transfers between devices: 5.34 us -> 52.9 us
  between operations: 13.3 us -> 0.37 us
  local copies, waits for them, and re-layouts: 19.1 us -> 31.9 us
  other arithmetic: 1.39 us -> 8.87 us
    unnamed x6 -> x0, waiting for transfers between devices: 169 us -> none
    all_gather x2 -> x0, waiting for transfers between devices: 106 us -> none  [sublayer(): lax.all_gather(hidden, RA, axis=0, tiled=True)]
    all_to_all x1 -> x6, waiting for transfers between devices: 12.1 us -> 75.6 us  [exchange(): return lax.all_to_all(parts, axes, 0, 0, tiled=True)]
    all_to_all x3 -> x6, blocking collectives: 55.8 us -> 119 us  [exchange(): return lax.all_to_all(parts, axes, 0, 0, tiled=True)]
    all_to_all x1 -> x6, starting transfers between devices: 5.26 us -> 32.1 us  [exchange(): return lax.all_to_all(parts, axes, 0, 0, tiled=True)]
    ppermute x0 -> x3, starting transfers between devices: none -> 20.8 us  [swap_core(): return lax.ppermute(block, 'c', [(0, 1), (1, 0)])]
    all_gather x0 -> x1, blocking collectives: none -> 18.8 us  [per_device(): affine = lax.all_gather(affine, 'x', axis=1, tiled=True)]
    slice x2 -> x7, local copies, waits for them, and re-layouts: 0.01 us -> 10.7 us  [the longest x3 6.95 us: per_device(): gu1, down1 = regroup_weights(gate_weight[1], up_weight[1], down_weight[1])]
  transfers between devices with their start and end apart: 5 -> 9, of which waited for: 5 -> 6; matrix products, arithmetic and copies ran while one was open for 0% -> 6% of each run, Pallas kernels for 0% -> 0%
where the time goes in v1:
time: 367 us; the launch traced here: 366 us
  blocking collectives  177 us (48%)
  waiting for transfers between devices  76.9 us (21%)
  starting transfers between devices  52.9 us (14%)
  local copies, waits for them, and re-layouts  31.9 us (9%)
  matrix products  18.1 us (5%)
  other arithmetic  8.87 us (2%)
    all_to_all x6, blocking collectives, exchange(): return lax.all_to_all(parts, axes, 0, 0, tiled=True)  119 us
    all_to_all x6, waiting for transfers between devices, exchange(): return lax.all_to_all(parts, axes, 0, 0, tiled=True)  75.6 us
    all_to_all x6, starting transfers between devices, exchange(): return lax.all_to_all(parts, axes, 0, 0, tiled=True)  32.1 us
    psum x1, blocking collectives, per_device(): lax.psum(jnp.stack((mixed.sum(axis=1), (mixed * mixed).sum(axis=1))), ('z...  31.9 us
    ppermute x3, starting transfers between devices, swap_core(): return lax.ppermute(block, 'c', [(0, 1), (1, 0)])  20.8 us
    all_gather x1, blocking collectives, per_device(): affine = lax.all_gather(affine, 'x', axis=1, tiled=True)  18.8 us
    dot_general x2, matrix products, dot_nt(): lax.dot_general(a, b, (((1,), (1,)), ((), ())), preferred_element_type=F32)  9.85 us
  transfers between devices with their start and end apart: 9, of which 6 were waited for; matrix products, arithmetic and copies ran while one was open for 6% of the time, Pallas kernels for 0%

profile of v1, /device:TPU:1, one launch (start us, length us, event | category | flops | bytes accessed | tf_op | source)
XLA Modules:
  0.0 365.9 jit_solution(2115882943331297913)
XLA Ops:
  0.0 2.4 fusion.6
  2.7 2.3 fusion.7
  5.2 2.3 fusion.8
  7.9 30.5 %all_to_all.60 = bf16[4,3,352,256]{3,2,1,0:T(8,128)(2,1)S(1)} all-to-all(bf16[4,3,352,256]{3,2,1,0:T(8,128)(2,1)S(1)} %copy.30), channel_id=1, replica_groups=mesh['z'=4,'x'=4,'y'=4,'c'=2] {'x'}, dimensions={0} | all-to-all | bytes 4325376 | tf_op jit(solution)/shard_map/all_to_all | solution.py:14
  38.7 2.2 collective-permute-start
  41.0 10.2 %all_to_all.61 = bf16[4,192,256]{2,1,0:T(8,128)(2,1)S(1)} all-to-all(bf16[4,192,256]{2,1,0:T(8,128)(2,1)S(1)} %broadcast_in_dim.14), channel_id=1, replica_groups=mesh['z'=4,'x'=4,'y'=4,'c'=2] {'x'}, dimensions={0} | all-to-all | bytes 786432 | tf_op jit(solution)/shard_map/all_to_all | solution.py:14
  52.7 4.4 %all-to-all-start.1 = ((bf16[4,192,1024]{2,1,0:T(8,128)(2,1)}), bf16[4,192,1024]{2,1,0:T(8,128)(2,1)}, u32[]{:S(2)}, u32[]{:S(2)}) async-start(bf16[4,192,1024]{2,1,0:T(8,128)(2,1)} %broadcast_in_dim.16), calls=%async_computation.1 | async-start | bytes 3145728 | tf_op jit(solution)/shard_map/all_to_all | solution.py:14
  59.0 2.0 copy-done.2
  62.9 13.6 %all-to-all-done.1 = bf16[4,192,1024]{2,1,0:T(8,128)(2,1)} async-done(((bf16[4,192,1024]{2,1,0:T(8,128)(2,1)}), bf16[4,192,1024]{2,1,0:T(8,128)(2,1)}, u32[]{:S(2)}, u32[]{:S(2)}) %all-to-all-start.1) | async-done | bytes 1572896 | tf_op jit(solution)/shard_map/all_to_all | solution.py:14
  76.5 4.9 %convolution_convert_fusion.1 = bf16[768,1408]{1,0:T(8,128)(2,1)S(1)} fusion(bf16[768,1024]{1,0:T(8,128)(2,1)} %bitcast.1, bf16[1408,1024]{1,0:T(8,128)(2,1)} %bitcast.85), kind=kOutput, calls=%fused_computation.3 | convolution fusion | flops 2215673856 | bytes 6619136 | tf_op jit(solution)/shard_map/dot_general | solution.py:26
  81.5 29.2 %all_to_all.62 = bf16[4,192,1408]{2,1,0:T(8,128)(2,1)S(1)} all-to-all(bf16[4,192,1408]{2,1,0:T(8,128)(2,1)S(1)} %bitcast.93), channel_id=1, replica_groups=mesh['z'=4,'x'=4,'y'=4,'c'=2] {'z'}, dimensions={0} | all-to-all | bytes 4325376 | tf_op jit(solution)/shard_map/all_to_all | solution.py:14
  112.4 4.4 %all-to-all-start.4 = ((bf16[4,192,704]{2,1,0:T(8,128)(2,1)}), bf16[4,192,704]{2,1,0:T(8,128)(2,1)}, u32[]{:S(2)}, u32[]{:S(2)}) async-start(bf16[4,192,704]{2,1,0:T(8,128)(2,1)} %broadcast_in_dim.17), calls=%async_computation.4 | async-start | bytes 2359296 | tf_op jit(solution)/shard_map/all_to_all | solution.py:14
  119.1 10.4 %all-to-all-done.4 = bf16[4,192,704]{2,1,0:T(8,128)(2,1)} async-done(((bf16[4,192,704]{2,1,0:T(8,128)(2,1)}), bf16[4,192,704]{2,1,0:T(8,128)(2,1)}, u32[]{:S(2)}, u32[]{:S(2)}) %all-to-all-start.4) | async-done | bytes 1081376 | tf_op jit(solution)/shard_map/all_to_all | solution.py:14
  129.5 3.6 all-to-all-start.7
  133.2 4.3 %convolution_convert_fusion.3 = bf16[768,1024]{1,0:T(8,128)(2,1)} fusion(bf16[768,704]{1,0:T(8,128)(2,1)} %bitcast.13, bf16[3,704,1024]{2,1,0:T(8,128)(2,1)} %copy-done.2), kind=kOutput, calls=%fused_computation.9 | convolution fusion | flops 1108082688 | bytes 4194304 | tf_op jit(solution)/shard_map/dot_general | solution.py:70
  137.5 18.0 %all-to-all-done.7 = bf16[4,3,352,256]{3,2,1,0:T(8,128)(2,1)S(1)} async-done(((bf16[4,3,352,256]{3,2,1,0:T(8,128)(2,1)}), bf16[4,3,352,256]{3,2,1,0:T(8,128)(2,1)S(1)}, u32[]{:S(2)}, u32[]{:S(2)}) %all-to-all-start.7) | async-done | bytes 2162720 | tf_op jit(solution)/shard_map/all_to_all | solution.py:14
  155.5 4.4 %all-to-all-start.5 = ((bf16[16,48,1024]{2,1,0:T(8,128)(2,1)}), bf16[16,48,1024]{2,1,0:T(8,128)(2,1)}, u32[]{:S(2)}, u32[]{:S(2)}) async-start(bf16[16,48,1024]{2,1,0:T(8,128)(2,1)} %bitcast.95), calls=%async_computation.5 | async-start | bytes 3145728 | tf_op jit(solution)/shard_map/all_to_all | solution.py:14
  160.0 18.8 %all_gather.3 = f32[2,1024]{1,0:T(2,128)S(1)} all-gather(f32[2,256]{1,0:T(2,128)S(1)} %pad_maximum_fusion), channel_id=1, replica_groups=mesh['z'=4,'x'=4,'y'=4,'c'=2] {'x'}, dimensions={1}, use_global_device_ids=true | all-gather | bytes 10240 | tf_op jit(solution)/shard_map/all_gather | solution.py:65
  180.4 8.3 %collective-permute-start.1 = (bf16[3,352,1024]{2,1,0:T(8,128)(2,1)}, bf16[3,352,1024]{2,1,0:T(8,128)(2,1)S(1)}, u32[]{:S(2)}, u32[]{:S(2)}) collective-permute-start(bf16[3,352,1024]{2,1,0:T(8,128)(2,1)} %bitcast.59), channel_id=1, source_target_pairs={{0,1},{1,0},{2,3},{3,2},{4,5},{5,4},{6,7},{7,6},{8,9},{9,8},{10,11... | collective-permute-start | bytes 6488072 | tf_op jit(solution)/shard_map/ppermute | solution.py:22
  191.5 6.9 %psum.14 = f32[2,48]{1,0:T(2,128)S(1)} all-reduce(f32[2,48]{1,0:T(2,128)S(1)} %pad_maximum_fusion.2), channel_id=1, replica_groups=mesh['z'=4,'x'=4,'y'=4,'c'=2] {'z'}, use_global_device_ids=true, to_apply=%region_4.5 | all-reduce | flops 96 | bytes 768 | tf_op jit(solution)/shard_map/psum | solution.py:75
  200.8 5.1 %all-to-all-start.6 = ((bf16[16,48,1024]{2,1,0:T(8,128)(2,1)}), bf16[16,48,1024]{2,1,0:T(8,128)(2,1)}, u32[]{:S(2)}, u32[]{:S(2)}) async-start(bf16[16,48,1024]{2,1,0:T(8,128)(2,1)} %broadcast_in_dim.18), calls=%async_computation.6 | async-start | bytes 3145728 | tf_op jit(solution)/shard_map/all_to_all | solution.py:14
  211.8 14.5 %all-to-all-done.6 = bf16[16,48,1024]{2,1,0:T(8,128)(2,1)} async-done(((bf16[16,48,1024]{2,1,0:T(8,128)(2,1)}), bf16[16,48,1024]{2,1,0:T(8,128)(2,1)}, u32[]{:S(2)}, u32[]{:S(2)}) %all-to-all-start.6) | async-done | bytes 1572896 | tf_op jit(solution)/shard_map/all_to_all | solution.py:14
  226.3 4.9 %convolution_convert_fusion = bf16[768,1408]{1,0:T(8,128)(2,1)S(1)} fusion(bf16[768,1024]{1,0:T(8,128)(2,1)} %bitcast.22, bf16[1408,1024]{1,0:T(8,128)(2,1)} %bitcast.86), kind=kOutput, calls=%fused_computation.2 | convolution fusion | flops 2215673856 | bytes 6619136 | tf_op jit(solution)/shard_map/dot_general | solution.py:26
  231.3 25.4 %all_to_all.63 = bf16[4,192,1408]{2,1,0:T(8,128)(2,1)S(1)} all-to-all(bf16[4,192,1408]{2,1,0:T(8,128)(2,1)S(1)} %bitcast.94), channel_id=1, replica_groups=mesh['z'=4,'x'=4,'y'=4,'c'=2] {'z'}, dimensions={0} | all-to-all | bytes 4325376 | tf_op jit(solution)/shard_map/all_to_all | solution.py:14
  257.4 13.7 %all_to_all.64 = bf16[4,192,704]{2,1,0:T(8,128)(2,1)S(1)} all-to-all(bf16[4,192,704]{2,1,0:T(8,128)(2,1)S(1)} %broadcast_in_dim.19), channel_id=1, replica_groups=mesh['z'=4,'x'=4,'y'=4,'c'=2] {'z'}, dimensions={0} | all-to-all | bytes 2162688 | tf_op jit(solution)/shard_map/all_to_all | solution.py:14
  271.1 3.9 %convolution_convert_fusion.2 = bf16[768,1024]{1,0:T(8,128)(2,1)} fusion(bf16[768,704]{1,0:T(8,128)(2,1)S(1)} %bitcast.100, bf16[3,704,1024]{2,1,0:T(8,128)(2,1)} %copy-done.3), kind=kOutput, calls=%fused_computation.8 | convolution fusion | flops 1108082688 | bytes 4096000 | tf_op jit(solution)/shard_map/dot_general | solution.py:80
  275.0 2.9 reshape.113
  279.3 10.2 %all-to-all-start.10 = ((bf16[16,192,256]{2,1,0:T(8,128)(2,1)}), bf16[16,192,256]{2,1,0:T(8,128)(2,1)S(1)}, u32[]{:S(2)}, u32[]{:S(2)}) async-start(bf16[16,192,256]{2,1,0:T(8,128)(2,1)} %bitcast.84), calls=%async_computation.10 | async-start | bytes 3145728 | tf_op jit(solution)/shard_map/all_to_all | solution.py:14
  289.6 19.0 %all-to-all-done.10 = bf16[16,192,256]{2,1,0:T(8,128)(2,1)S(1)} async-done(((bf16[16,192,256]{2,1,0:T(8,128)(2,1)}), bf16[16,192,256]{2,1,0:T(8,128)(2,1)S(1)}, u32[]{:S(2)}, u32[]{:S(2)}) %all-to-all-start.10) | async-done | bytes 1572896 | tf_op jit(solution)/shard_map/all_to_all | solution.py:14
  309.9 31.9 %psum.15 = f32[2,192]{1,0:T(2,128)S(1)} all-reduce(f32[2,192]{1,0:T(2,128)S(1)} %pad_maximum_fusion.1), channel_id=1, replica_groups=mesh['z'=4,'x'=4,'y'=4,'c'=2] {'z','x'}, use_global_device_ids=true, to_apply=%region_9.10 | all-reduce | flops 384 | bytes 3072 | tf_op jit(solution)/shard_map/psum | solution.py:85
  342.9 10.1 %all_to_all.65 = bf16[4,192,256]{2,1,0:T(8,128)(2,1)S(1)} all-to-all(bf16[4,192,256]{2,1,0:T(8,128)(2,1)S(1)} %broadcast_in_dim.20), channel_id=1, replica_groups=mesh['z'=4,'x'=4,'y'=4,'c'=2] {'y'}, dimensions={0} | all-to-all | bytes 786432 | tf_op jit(solution)/shard_map/all_to_all | solution.py:14
  353.0 10.3 %collective-permute-start.2 = (bf16[768,256]{1,0:T(8,128)(2,1)S(1)}, bf16[768,256]{1,0:T(8,128)(2,1)S(1)}, u32[]{:S(2)}, u32[]{:S(2)}) collective-permute-start(bf16[768,256]{1,0:T(8,128)(2,1)S(1)} %bitcast.97), channel_id=1, source_target_pairs={{0,1},{1,0},{2,3},{3,2},{4,5},{5,4},{6,7},{7,6},{8,9},{9,8},{10,11... | collective-permute-start | bytes 1179656 | tf_op jit(solution)/shard_map/ppermute | solution.py:22
  (66 shorter events, 30.2 us)
Async XLA Ops:
  0.0 40.9 %copy-start = (bf16[1536,256]{1,0:T(8,128)(2,1)S(1)}, bf16[1536,256]{1,0:T(8,128)(2,1)}, u32[]{:S(2)}) copy-start(bf16[1536,256]{1,0:T(8,128)(2,1)} %param.6) | copy-start | bytes 2359300
  38.7 18.5 %collective-permute-start = (bf16[3,352,1024]{2,1,0:T(8,128)(2,1)S(1)}, bf16[3,352,1024]{2,1,0:T(8,128)(2,1)}, u32[]{:S(2)}, u32[]{:S(2)}) collective-permute-start(bf16[3,352,1024]{2,1,0:T(8,128)(2,1)S(1)} %bitcast.81), channel_id=1, source_target_pairs={{0,1},{1,0},{2,3},{3,2},{4,5},{5,4},{6,7},{7,6},{8,9},{9,8},{10,11... | collective-permute-start | bytes 6488072 | tf_op jit(solution)/shard_map/ppermute | solution.py:22
  52.7 23.9 %all-to-all-start.1 = ((bf16[4,192,1024]{2,1,0:T(8,128)(2,1)}), bf16[4,192,1024]{2,1,0:T(8,128)(2,1)}, u32[]{:S(2)}, u32[]{:S(2)}) async-start(bf16[4,192,1024]{2,1,0:T(8,128)(2,1)} %broadcast_in_dim.16), calls=%async_computation.1 | async-start | bytes 3145728 | tf_op jit(solution)/shard_map/all_to_all | solution.py:14
  59.0 2.1 copy-start.2
  111.2 5.6 %copy-start.4 = (bf16[1,256,1408]{2,1,0:T(8,128)(2,1)S(1)}, bf16[1,256,1408]{2,1,0:T(8,128)(2,1)}, u32[]{:S(2)}) copy-start(bf16[1,256,1408]{2,1,0:T(8,128)(2,1)} %get-tuple-element.9) | copy-start | bytes 2162692
  112.4 4.7 %copy-start.5 = (bf16[1,256,1408]{2,1,0:T(8,128)(2,1)S(1)}, bf16[1,256,1408]{2,1,0:T(8,128)(2,1)}, u32[]{:S(2)}) copy-start(bf16[1,256,1408]{2,1,0:T(8,128)(2,1)} %get-tuple-element.11) | copy-start | bytes 2162692
  112.4 5.0 %copy-start.6 = (bf16[1,1408,256]{2,1,0:T(8,128)(2,1)S(1)}, bf16[1,1408,256]{2,1,0:T(8,128)(2,1)}, u32[]{:S(2)}) copy-start(bf16[1,1408,256]{2,1,0:T(8,128)(2,1)} %get-tuple-element.13) | copy-start | bytes 2162692
  112.4 17.1 %all-to-all-start.4 = ((bf16[4,192,704]{2,1,0:T(8,128)(2,1)}), bf16[4,192,704]{2,1,0:T(8,128)(2,1)}, u32[]{:S(2)}, u32[]{:S(2)}) async-start(bf16[4,192,704]{2,1,0:T(8,128)(2,1)} %broadcast_in_dim.17), calls=%async_computation.4 | async-start | bytes 2359296 | tf_op jit(solution)/shard_map/all_to_all | solution.py:14
  129.5 25.9 %all-to-all-start.7 = ((bf16[4,3,352,256]{3,2,1,0:T(8,128)(2,1)}), bf16[4,3,352,256]{3,2,1,0:T(8,128)(2,1)S(1)}, u32[]{:S(2)}, u32[]{:S(2)}) async-start(bf16[4,3,352,256]{3,2,1,0:T(8,128)(2,1)} %copy.34), calls=%async_computation.7 | async-start | bytes 4325376 | tf_op jit(solution)/shard_map/all_to_all | solution.py:14
  137.5 22.4 %copy-start.7 = (f32[2,256]{1,0:T(2,128)S(1)}, f32[2,256]{1,0:T(2,128)}, u32[]{:S(2)}) copy-start(f32[2,256]{1,0:T(2,128)} %param.10) | copy-start | bytes 6148
  137.5 22.5 %copy-start.8 = (f32[2,256]{1,0:T(2,128)S(1)}, f32[2,256]{1,0:T(2,128)}, u32[]{:S(2)}) copy-start(f32[2,256]{1,0:T(2,128)} %param.11) | copy-start | bytes 6148
  155.5 33.3 %all-to-all-start.5 = ((bf16[16,48,1024]{2,1,0:T(8,128)(2,1)}), bf16[16,48,1024]{2,1,0:T(8,128)(2,1)}, u32[]{:S(2)}, u32[]{:S(2)}) async-start(bf16[16,48,1024]{2,1,0:T(8,128)(2,1)} %bitcast.95), calls=%async_computation.5 | async-start | bytes 3145728 | tf_op jit(solution)/shard_map/all_to_all | solution.py:14
  180.4 27.2 %collective-permute-start.1 = (bf16[3,352,1024]{2,1,0:T(8,128)(2,1)}, bf16[3,352,1024]{2,1,0:T(8,128)(2,1)S(1)}, u32[]{:S(2)}, u32[]{:S(2)}) collective-permute-start(bf16[3,352,1024]{2,1,0:T(8,128)(2,1)} %bitcast.59), channel_id=1, source_target_pairs={{0,1},{1,0},{2,3},{3,2},{4,5},{5,4},{6,7},{7,6},{8,9},{9,8},{10,11... | collective-permute-start | bytes 6488072 | tf_op jit(solution)/shard_map/ppermute | solution.py:22
  200.8 25.5 %all-to-all-start.6 = ((bf16[16,48,1024]{2,1,0:T(8,128)(2,1)}), bf16[16,48,1024]{2,1,0:T(8,128)(2,1)}, u32[]{:S(2)}, u32[]{:S(2)}) async-start(bf16[16,48,1024]{2,1,0:T(8,128)(2,1)} %broadcast_in_dim.18), calls=%async_computation.6 | async-start | bytes 3145728 | tf_op jit(solution)/shard_map/all_to_all | solution.py:14
  207.9 2.0 copy-start.3
  279.3 29.2 %all-to-all-start.10 = ((bf16[16,192,256]{2,1,0:T(8,128)(2,1)}), bf16[16,192,256]{2,1,0:T(8,128)(2,1)S(1)}, u32[]{:S(2)}, u32[]{:S(2)}) async-start(bf16[16,192,256]{2,1,0:T(8,128)(2,1)} %bitcast.84), calls=%async_computation.10 | async-start | bytes 3145728 | tf_op jit(solution)/shard_map/all_to_all | solution.py:14
  308.6 57.3 %copy-start.1 = (bf16[1536,256]{1,0:T(8,128)(2,1)S(1)}, bf16[1536,256]{1,0:T(8,128)(2,1)}, u32[]{:S(2)}) copy-start(bf16[1536,256]{1,0:T(8,128)(2,1)} %param.6) | copy-start | bytes 2359300
  353.0 11.7 %collective-permute-start.2 = (bf16[768,256]{1,0:T(8,128)(2,1)S(1)}, bf16[768,256]{1,0:T(8,128)(2,1)S(1)}, u32[]{:S(2)}, u32[]{:S(2)}) collective-permute-start(bf16[768,256]{1,0:T(8,128)(2,1)S(1)} %bitcast.97), channel_id=1, source_target_pairs={{0,1},{1,0},{2,3},{3,2},{4,5},{5,4},{6,7},{7,6},{8,9},{9,8},{10,11... | collective-permute-start | bytes 1179656 | tf_op jit(solution)/shard_map/ppermute | solution.py:22
